TPU v7x, 32 devices: a whole 2x2x4 slice. The times are simulated.
32 devices in a mesh: sp: 8 (over z, x), tp: 4 (over y, core).
Axes of the slice: x: 2, y: 2, z: 4, core: 2. Of those that a mesh axis runs over, the one named last changes fastest.
Arguments:
- residual: bfloat16 [1536, 2048], P('sp', 'tp'), may hold values from -10 to 10
- queries: bfloat16 [1536, 16, 128], P('sp', 'tp'), may hold values from -6.5 to 6.5
- key_rows: bfloat16 [1536, 16, 128], P('sp', 'tp'), may hold values from -6.5 to 6.5
- value_rows: bfloat16 [1536, 16, 128], P('sp', 'tp'), may hold values from -6 to 6
- diff_scale: float32 [16], P('tp'), may hold values from 0.3 to 0.8
- head_gain: float32 [128], replicated, may hold values from 0.1 to 1.9
- out_weight: bfloat16 [2048, 2048], P(None, 'tp'), may hold values from -0.125 to 0.125
- norm_gain: float32 [2048], replicated, may hold values from 0.1 to 1.9
- gate_weight: bfloat16 [8, 2048, 4096], P('sp', None, 'tp'), may hold values from -0.5 to 0.5
- up_weight: bfloat16 [8, 2048, 4096], P('sp', None, 'tp'), may hold values from -0.5 to 0.5
- down_weight: bfloat16 [8, 4096, 2048], P('sp', None, 'tp'), may hold values from -0.01171875 to 0.01171875
- expert_ids: int32 [1536, 2], P('sp'), may hold values from 0 to 7, all different within a row; in each aligned block of 192 rows (0 to 191, 192 to 383, ...) at most 96 rows name the same one
- route_logit: float32 [1536, 2], P('sp'), may hold values from -6 to 6
Outputs:
- updated: bfloat16 [1536, 2048], P('sp', 'tp')
Inputs may be any that keep to these rules, and one draw needn't show every extreme that they name: `expert_ids`: A token's 2 experts differ. The 192 tokens of one index of sp name one expert at most 96 times, a bound that some block reaches on some index.
All inputs are finite; a program needn't handle non-finite values.
Results may differ from a plain program's by a relative error of at most 0.014.
Values may be sent and summed in bfloat16 or wider, within the bound.
A program may use at most 64 MiB of HBM per device.

v0:
```python
import math

import jax
import jax.numpy as jnp
from jax import lax
from jax.sharding import PartitionSpec as P

D = 2048
QK = 64
SPAN = 64


NORM_EPS = 1e-05
CLAMP_LIMIT = 7.0
SWISH_ALPHA = 1.702
HEAD_KEEP = 0.8
NEG_FILL = -1e30


def update_map(running, query_half, key_half, value_block, visible):
    row_peak, row_total, accum = running
    scores = jnp.einsum(
        "qhd,khd->hqk", query_half, key_half, preferred_element_type=jnp.float32
    ) * QK ** (-0.5)
    scores = jnp.where(visible[None], scores, NEG_FILL)
    new_peak = jnp.maximum(row_peak, jnp.max(scores, axis=-1))
    exp_weights = jnp.where(visible[None], jnp.exp(scores - new_peak[..., None]), 0.0)
    rescale = jnp.exp(row_peak - new_peak)
    row_total = row_total * rescale + jnp.sum(exp_weights, axis=-1)
    accum = accum * rescale[..., None] + jnp.einsum(
        "hqk,khv->hqv",
        exp_weights.astype(jnp.bfloat16),
        value_block,
        preferred_element_type=jnp.float32,
    )
    return (new_peak, row_total, accum)


def local(
    residual,
    queries,
    key_rows,
    value_rows,
    diff_scale,
    head_gain,
    out_weight,
    norm_gain,
    gate_weight,
    up_weight,
    down_weight,
    expert_ids,
    route_logit,
):
    tokens_here = queries.shape[0]
    heads_here = queries.shape[1]
    value_width = value_rows.shape[2]
    query_start = lax.axis_index("sp") * tokens_here
    query_span = (query_start + jnp.arange(tokens_here, dtype=jnp.int32)) // SPAN
    first_query = queries[..., :QK]
    second_query = queries[..., QK:]
    empty_map = (
        jnp.full((heads_here, tokens_here), NEG_FILL, jnp.float32),
        jnp.zeros((heads_here, tokens_here), jnp.float32),
        jnp.zeros((heads_here, tokens_here, value_width), jnp.float32),
    )
    folded = (empty_map, empty_map)
    key_piece = lax.all_gather(key_rows, "sp", axis=0, tiled=True)
    value_piece = lax.all_gather(value_rows, "sp", axis=0, tiled=True)
    key_count = key_piece.shape[0]
    key_width = math.gcd(key_count, 1024)
    blocks = key_count // key_width
    key_blocks = key_piece.reshape(blocks, key_width, heads_here, 2 * QK)
    value_blocks = value_piece.reshape(blocks, key_width, heads_here, value_width)

    def advance(running, inputs):
        block_index, key_block, value_block = inputs
        key_start = block_index * key_width

        def compute(current):
            key_span = (key_start + jnp.arange(key_width, dtype=jnp.int32)) // SPAN
            visible = key_span[None, :] <= query_span[:, None]
            first = update_map(current[0], first_query, key_block[..., :QK], value_block, visible)
            second = update_map(current[1], second_query, key_block[..., QK:], value_block, visible)
            return (first, second)

        running = lax.cond(
            key_start < query_start + tokens_here, compute, lambda current: current, running
        )
        return (running, None)

    folded, _ = lax.scan(
        advance, folded, (jnp.arange(blocks, dtype=jnp.int32), key_blocks, value_blocks)
    )
    first_map, second_map = folded
    mixture = (
        first_map[2] / first_map[1][..., None]
        - diff_scale[:, None, None] * second_map[2] / second_map[1][..., None]
    )
    scale_back = lax.rsqrt(jnp.mean(mixture * mixture, axis=-1, keepdims=True) + NORM_EPS)
    attended = (mixture * scale_back * head_gain * HEAD_KEEP).astype(jnp.bfloat16)
    column_width = out_weight.shape[1]
    head_weight = out_weight.reshape(-1, value_width, column_width)
    weight_slice = head_weight
    projected = jnp.einsum(
        "htv,hvd->td",
        lax.all_gather(attended, "tp", axis=0, tiled=True),
        weight_slice,
        preferred_element_type=jnp.float32,
    )
    after_mixer = (residual.astype(jnp.float32) + projected).astype(jnp.bfloat16)
    mixer_float = after_mixer.astype(jnp.float32)
    partial_value = jnp.sum(mixer_float * mixer_float, axis=-1)
    square_total = lax.psum(partial_value, "tp")
    gain_slice = lax.dynamic_slice_in_dim(
        norm_gain, lax.axis_index("tp") * column_width, column_width, 0
    )
    normed = (mixer_float * lax.rsqrt(square_total / D + NORM_EPS)[:, None] * gain_slice).astype(
        jnp.bfloat16
    )
    experts = lax.axis_size("sp")
    top_count = expert_ids.shape[1]
    capacity = 2 * tokens_here * top_count // experts
    chosen = expert_ids.reshape(-1)
    onehot = (chosen[:, None] == jnp.arange(experts, dtype=jnp.int32)[None, :]).astype(jnp.int32)
    rank_in = jnp.sum(jnp.cumsum(onehot, axis=0) * onehot, axis=1) - 1
    slot_index = chosen * capacity + rank_in
    owner_row = (
        jnp.full((experts * capacity,), tokens_here, jnp.int32)
        .at[slot_index]
        .set(jnp.arange(tokens_here * top_count, dtype=jnp.int32) // top_count)
    )
    padded = jnp.concatenate([normed, jnp.zeros((1, normed.shape[1]), jnp.bfloat16)], axis=0)
    outgoing = padded[owner_row].reshape(experts, capacity, normed.shape[1])
    expert_input = lax.all_gather(
        lax.all_to_all(outgoing, "sp", split_axis=0, concat_axis=0, tiled=True),
        "tp",
        axis=2,
        tiled=True,
    )
    sources = expert_input.shape[0]
    items = expert_input.shape[1]
    flat_rows = expert_input.reshape(sources * items, -1)
    pre_gate = jnp.dot(flat_rows, gate_weight[0], preferred_element_type=jnp.float32)
    pre_up = jnp.dot(flat_rows, up_weight[0], preferred_element_type=jnp.float32)
    capped = jnp.minimum(pre_gate, CLAMP_LIMIT)
    linear = jnp.clip(pre_up, -CLAMP_LIMIT, CLAMP_LIMIT)
    hidden = (capped * jax.nn.sigmoid(SWISH_ALPHA * capped) * (linear + 1.0)).astype(jnp.bfloat16)
    weight_slice = down_weight[0]
    expert_out = jnp.dot(
        lax.all_gather(hidden, "tp", axis=1, tiled=True),
        weight_slice,
        preferred_element_type=jnp.float32,
    )
    expert_out = expert_out.astype(jnp.bfloat16).reshape(sources, items, -1)
    returned_rows = lax.all_to_all(expert_out, "sp", split_axis=0, concat_axis=0, tiled=True)
    picked = returned_rows.reshape(experts * capacity, -1)[slot_index].astype(jnp.float32)
    picked = picked.reshape(tokens_here, top_count, -1)
    weights = jax.nn.softmax(route_logit, axis=-1)
    routed = jnp.sum(picked * weights[..., None], axis=1)
    return (mixer_float + routed).astype(jnp.bfloat16)


def solution(mesh):
    return jax.shard_map(
        local,
        mesh=mesh,
        in_specs=(
            P("sp", "tp"),
            P("sp", "tp", None),
            P("sp", "tp", None),
            P("sp", "tp", None),
            P("tp"),
            P(),
            P(None, "tp"),
            P(),
            P("sp", None, "tp"),
            P("sp", None, "tp"),
            P("sp", None, "tp"),
            P("sp", None),
            P("sp", None),
        ),
        out_specs=P("sp", "tp"),
        check_vma=False,
    )
```

profile of v0, /device:TPU:0, one launch (start us, length us, event | category | flops | bytes accessed | tf_op | source)
XLA Modules:
  0.0 296.3 jit_solution(3500172858010482587)
XLA Ops:
  6.5 1.8 copy.27
  8.4 0.0 all-gather.5.cloned.1.call-update
  8.4 0.0 all-gather.7.cloned.1.call-start
  8.4 1.6 copy.29
  10.1 0.0 all-gather.7.cloned.1.call-update
  10.1 0.0 all-gather.9.cloned.1.call-start
  10.1 0.8 copy.34
  10.9 0.1 eq.29
  11.1 0.1 eq.25
  11.2 0.0 copy-done.2
  11.2 0.2 fusion.56
  11.4 0.1 copy.37
  11.6 0.1 copy.38
  11.8 0.9 reduce-window.6
  12.6 0.2 slice_reduce_fusion
  12.9 0.1 copy.33
  13.0 0.1 mul.173
  13.2 0.8 dynamic_slice.28
  14.0 0.1 fusion.44
  14.1 2.9 scatter_custom_fusion
  17.0 39.5 %all-gather.5.cloned.1.call-done = bf16[1536,4,128]{2,0,1:T(8,128)(2,1)} async-done(((bf16[192,4,128]{2,0,1:T(8,128)(2,1)}), bf16[1536,4,128]{2,0,1:T(8,128)(2,1)}) %all-gather.5.cloned.1.call-update) | async-done | bytes 1572880 | tf_op jit(solution)/shard_map/all_gather | solution.py:67
  56.5 2.6 copy.31
  59.1 42.2 %all-gather.7.cloned.1.call-done = bf16[1536,4,128]{2,0,1:T(8,128)(2,1)} async-done(((bf16[192,4,128]{2,0,1:T(8,128)(2,1)}), bf16[1536,4,128]{2,0,1:T(8,128)(2,1)}) %all-gather.7.cloned.1.call-update) | async-done | bytes 1572880 | tf_op jit(solution)/shard_map/all_gather | solution.py:68
  101.2 2.7 copy.32
  104.0 0.0 copy-start.6
  104.0 0.0 copy-start.7
  104.0 9.0 %while.23 = (s32[]{:T(128)}, f32[4,192]{1,0:T(4,128)S(1)}, f32[4,192]{1,0:T(4,128)S(1)}, f32[4,192,128]{2,1,0:T(8,128)S(1)}, f32[4,192]{1,0:T(4,128)S(1)}, /*ind...) while((s32[]{:T(128)}, f32[4,192]{1,0:T(4,128)S(1)}, ...), condition=%wide.region_7.8_spmd.clone, body=%wide.region_0.7_spmd.clone.sunk | while | flops 309574784 | bytes 20891532 | solution.py:91
  104.1 0.6 dynamic_slice.42
  105.4 5.0 %conditional.3 = ((f32[4,192]{1,0:T(4,128)S(1)}, f32[4,192]{1,0:T(4,128)S(1)}, f32[4,192,128]{2,1,0:T(8,128)S(1)}, f32[4,192]{1,0:T(4,128)S(1)}, f32[4,192]{1,0:T(4,128)S(1)}, /*index=5*/f32[4,192,128]{2,1,0:T(8,128)S(1)})) conditional(s32[]{:T(128)} %convert_element_type.82, (f32[4,192]{1,0:T(4,128)S(1)}, f32[4,192]{1,0:T(4,128)S(1)}, ...), branch_computations={%region_1.1_spmd, %region_2.6_spmd.clone} | conditional | flops 309572096 | bytes 20887848 | solution.py:86
  105.4 0.1 broadcast_compare_fusion
  105.5 1.1 dynamic-slice_bitcast_fusion
  106.6 0.6 fusion.54
  107.2 0.6 fusion.55
  107.8 1.2 fusion.5
  109.0 0.2 copy-done.1
  109.2 0.6 convolution_add_fusion
  109.7 0.6 convolution_add_fusion.1
  110.4 0.6 dynamic_slice.42
  111.7 0.6 dynamic_slice.42
  113.0 0.0 copy-start.3
  113.0 0.0 copy-done.6
  113.1 0.5 multiply_reduce_fusion.2
  113.6 0.2 multiply_convert_fusion.2
  113.7 8.6 %all_gather.17 = bf16[16,192,128]{2,1,0:T(8,128)(2,1)S(1)} all-gather(bf16[4,192,128]{2,1,0:T(8,128)(2,1)S(1)} %multiply_convert_fusion.2), channel_id=1, replica_groups=mesh['sp'=8,'tp'=4] {'tp'}, dimensions={0}, use_global_device_ids=true | all-gather | bytes 983040 | tf_op jit(solution)/shard_map/all_gather | solution.py:106
  122.3 0.7 multiply_reduce_fusion.1
  123.0 6.2 %psum.7 = f32[192]{0:T(256)S(1)} all-reduce(f32[192]{0:T(256)S(1)} %get-tuple-element.467), channel_id=1, replica_groups=mesh['sp'=8,'tp'=4] {'tp'}, use_global_device_ids=true, to_apply=%region_10.11 | all-reduce | flops 192 | bytes 1536 | tf_op jit(solution)/shard_map/psum | solution.py:113
  129.2 0.1 multiply_convert_fusion.1
  129.3 2.7 gather_fusion
  132.0 32.5 %all_to_all.10 = bf16[8,96,512]{2,1,0:T(8,128)(2,1)} all-to-all(bf16[8,96,512]{2,1,0:T(8,128)(2,1)S(1)} %bitcast.62), channel_id=1, replica_groups=mesh['sp'=8,'tp'=4] {'sp'}, dimensions={0} | all-to-all | bytes 1572864 | tf_op jit(solution)/shard_map/all_to_all | solution.py:135
  164.5 0.0 all-gather.9.cloned.1.call-update
  164.5 0.2 all-gather.11.cloned.1.call-start
  164.7 26.5 %all-gather.9.cloned.1.call-done = bf16[8,96,2048]{2,1,0:T(8,128)(2,1)} async-done(((bf16[8,96,512]{2,1,0:T(8,128)(2,1)}), bf16[8,96,2048]{2,1,0:T(8,128)(2,1)}) %all-gather.9.cloned.1.call-update) | async-done | bytes 3145744 | tf_op jit(solution)/shard_map/all_gather | solution.py:134
  191.3 6.3 %fusion.32 = f32[768,1024]{1,0:T(8,128)S(1)} fusion(bf16[768,2048]{1,0:T(8,128)(2,1)} %bitcast.67, bf16[1,2048,1024]{2,1,0:T(8,128)(2,1)} %param.26), kind=kOutput, calls=%fused_computation.55 | convolution fusion | flops 3221225472 | bytes 10485760 | tf_op jit(solution)/shard_map/dot_general | solution.py:144
  197.6 5.3 %multiply_convert_fusion = bf16[768,1024]{1,0:T(8,128)(2,1)} fusion(f32[768,1024]{1,0:T(8,128)S(1)} %fusion.32, bf16[768,2048]{1,0:T(8,128)(2,1)S(1)} %bitcast.68, bf16[1,2048,1024]{2,1,0:T(8,128)(2,1)S(1)} %copy-done.8), kind=kOutput, calls=%fused_computation.59 | convolution fusion | flops 3229089792 | bytes 12058624 | tf_op jit(solution)/shard_map/dot_general | solution.py:143
  202.9 0.0 all-gather.11.cloned.1.call-update
  202.9 46.5 %all-gather.11.cloned.1.call-done = bf16[768,4096]{1,0:T(8,128)(2,1)} async-done(((bf16[768,1024]{1,0:T(8,128)(2,1)}), bf16[768,4096]{1,0:T(8,128)(2,1)}) %all-gather.11.cloned.1.call-update) | async-done | bytes 6291472 | tf_op jit(solution)/shard_map/all_gather | solution.py:150
  249.4 8.3 %fusion.38 = bf16[768,512]{1,0:T(8,128)(2,1)} fusion(bf16[768,4096]{1,0:T(8,128)(2,1)} %all-gather.11.cloned.1.call-done, bf16[1,4096,512]{2,1,0:T(8,128)(2,1)} %param.27), kind=kOutput, calls=%fused_computation.60 | convolution fusion | flops 3221618688 | bytes 11272192 | tf_op jit(solution)/shard_map/dot_general | solution.py:149
  257.7 5.6 %all-to-all-start.1 = ((bf16[8,96,512]{2,1,0:T(8,128)(2,1)}), bf16[8,96,512]{2,1,0:T(8,128)(2,1)S(1)}, u32[]{:S(2)}, u32[]{:S(2)}) async-start(bf16[8,96,512]{2,1,0:T(8,128)(2,1)} %bitcast.65), calls=%async_computation.1 | async-start | bytes 1572864 | tf_op jit(solution)/shard_map/all_to_all | solution.py:155
  263.4 0.1 copy.36
  263.6 20.4 %all-to-all-done.1 = bf16[8,96,512]{2,1,0:T(8,128)(2,1)S(1)} async-done(((bf16[8,96,512]{2,1,0:T(8,128)(2,1)}), bf16[8,96,512]{2,1,0:T(8,128)(2,1)S(1)}, u32[]{:S(2)}, u32[]{:S(2)}) %all-to-all-start.1) | async-done | bytes 786464 | tf_op jit(solution)/shard_map/all_to_all | solution.py:155
  283.9 2.6 gather_fusion.1
  286.5 1.5 reshape.153
  288.0 1.0 multiply_reduce_fusion
  289.0 0.7 add_convert_fusion
  (58 shorter events, 0.4 us)
Async XLA Ops:
  6.5 115.8 %copy-start = (bf16[2048,512]{1,0:T(8,128)(2,1)S(1)}, bf16[2048,512]{1,0:T(8,128)(2,1)}, u32[]{:S(2)}) copy-start(bf16[2048,512]{1,0:T(8,128)(2,1)} %param.23) | copy-start | bytes 6291460
  6.5 6.4 %copy-start.5 = (s32[192,2]{0,1:T(2,128)S(1)}, s32[192,2]{0,1:T(2,128)}, u32[]{:S(2)}) copy-start(s32[192,2]{0,1:T(2,128)} %param.28) | copy-start | bytes 4612
  6.5 4.7 %copy-start.2 = (bf16[192,4,128]{2,1,0:T(4,128)(2,1)S(1)}, bf16[192,4,128]{2,1,0:T(4,128)(2,1)}, u32[]{:S(2)}) copy-start(bf16[192,4,128]{2,1,0:T(4,128)(2,1)} %param.18) | copy-start | bytes 589828
  6.5 49.9 %all-gather.5.cloned.1.call-start = ((), (), s32[]{:S(2)}) async-start(), calls=%async_computation.2 | async-start | bytes 1769472 | tf_op jit(solution)/shard_map/all_gather | solution.py:67
  8.4 92.9 %all-gather.7.cloned.1.call-start = ((), (), s32[]{:S(2)}) async-start(), calls=%async_computation.3 | async-start | bytes 1769472 | tf_op jit(solution)/shard_map/all_gather | solution.py:68
  10.1 181.2 %all-gather.9.cloned.1.call-start = ((), (), s32[]{:S(2)}) async-start(), calls=%async_computation.4 | async-start | bytes 3932160 | tf_op jit(solution)/shard_map/all_gather | solution.py:134
  104.0 9.0 %copy-start.6 = (f32[4]{0:T(128)S(1)}, f32[4]{0:T(128)}, u32[]{:S(2)}) copy-start(f32[4]{0:T(128)} %param.21) | copy-start | bytes 52
  104.0 9.5 %copy-start.7 = (f32[128]{0:T(128)S(1)}, f32[128]{0:T(128)}, u32[]{:S(2)}) copy-start(f32[128]{0:T(128)} %param.22) | copy-start | bytes 1540
  107.8 1.4 copy-start.1
  113.0 9.3 %copy-start.3 = (bf16[192,512]{1,0:T(8,128)(2,1)S(1)}, bf16[192,512]{1,0:T(8,128)(2,1)}, u32[]{:S(2)}) copy-start(bf16[192,512]{1,0:T(8,128)(2,1)} %param.17) | copy-start | bytes 589828
  164.5 84.9 %all-gather.11.cloned.1.call-start = ((), (), s32[]{:S(2)}) async-start(), calls=%async_computation.5 | async-start | bytes 7864320 | tf_op jit(solution)/shard_map/all_gather | solution.py:150
  191.2 6.3 %copy-start.8 = (bf16[1,2048,1024]{2,1,0:T(8,128)(2,1)S(1)}, bf16[1,2048,1024]{2,1,0:T(8,128)(2,1)}, u32[]{:S(2)}) copy-start(bf16[1,2048,1024]{2,1,0:T(8,128)(2,1)} %param.25) | copy-start | bytes 12582916
  191.3 6.3 %copy-start.9 = (bf16[8,96,2048]{2,1,0:T(8,128)(2,1)S(1)}, bf16[8,96,2048]{2,1,0:T(8,128)(2,1)}, u32[]{:S(2)}) copy-start(bf16[8,96,2048]{2,1,0:T(8,128)(2,1)} %all-gather.9.cloned.1.call-done) | copy-start | bytes 9437188
  257.7 5.7 %copy-start.4 = (f32[192,2]{0,1:T(2,128)S(1)}, f32[192,2]{0,1:T(2,128)}, u32[]{:S(2)}) copy-start(f32[192,2]{0,1:T(2,128)} %param.29) | copy-start | bytes 4612
  257.7 26.2 %all-to-all-start.1 = ((bf16[8,96,512]{2,1,0:T(8,128)(2,1)}), bf16[8,96,512]{2,1,0:T(8,128)(2,1)S(1)}, u32[]{:S(2)}, u32[]{:S(2)}) async-start(bf16[8,96,512]{2,1,0:T(8,128)(2,1)} %bitcast.65), calls=%async_computation.1 | async-start | bytes 1572864 | tf_op jit(solution)/shard_map/all_to_all | solution.py:155
Sparse Core Ops, SparseCore 0:
  9.5 46.9 all-gather.4
  58.7 42.5 all-gather.6
  164.6 26.5 all-gather.8
  203.0 46.3 all-gather.10
where the time goes:
time: 297 us; the launch traced here: 296 us
  waiting for transfers between devices  175 us (59%)
  blocking collectives  47.2 us (16%)
  local copies, waits for them, and re-layouts  24.5 us (8%)
  matrix products  22.8 us (8%)
  between operations  13.4 us (5%)
  starting transfers between devices  5.96 us (2%)
  other arithmetic  5.09 us (2%)
    all_gather x1, waiting for transfers between devices, local(): lax.all_gather(hidden, 'tp', axis=1, tiled=True)  46.5 us
    all_gather x1, waiting for transfers between devices, local(): value_piece = lax.all_gather(value_rows, 'sp', axis=0, tiled=True)  42.2 us
    all_gather x1, waiting for transfers between devices, local(): key_piece = lax.all_gather(key_rows, 'sp', axis=0, tiled=True)  39.5 us
    all_to_all x1, blocking collectives, local(): lax.all_to_all(outgoing, 'sp', split_axis=0, concat_axis=0, tiled=True)  32.5 us
    all_gather x1, waiting for transfers between devices, local(): lax.all_gather(lax.all_to_all(outgoing, 'sp', split_axis=0, concat_axis=0...  26.5 us
    all_to_all x1, waiting for transfers between devices, local(): lax.all_to_all(expert_out, 'sp', split_axis=0, concat_axis=0, tiled=True)  20.4 us
    unnamed x25, local copies, waits for them, and re-layouts  9.82 us
    all_gather x1, blocking collectives, local(): lax.all_gather(attended, 'tp', axis=0, tiled=True)  8.58 us
  transfers between devices with their start and end apart: 5, of which 5 were waited for; matrix products, arithmetic and copies ran while one was open for 4% of the time, Pallas kernels for 0%

commit v1 on v0

--- a/solution.py
+++ b/solution.py
@@ -1,8 +1,11 @@
+import functools
 import math
 
 import jax
 import jax.numpy as jnp
 from jax import lax
+from jax.experimental import pallas as pl
+from jax.experimental.pallas import tpu as pltpu
 from jax.sharding import PartitionSpec as P
 
 D = 2048
@@ -34,6 +37,295 @@
         preferred_element_type=jnp.float32,
     )
     return (new_peak, row_total, accum)
+
+
+def expert_kernel(
+    sp_size,
+    tp_size,
+    groups,
+    outgoing,
+    gate_hbm,
+    up_hbm,
+    down_hbm,
+    returned,
+    rows_in,
+    hidden,
+    result,
+    gate,
+    up,
+    down,
+    weight_sem,
+    local_sem,
+    disp_send,
+    disp_recv,
+    ret_send,
+    ret_recv,
+    row_send,
+    row_recv,
+    hid_send,
+    hid_recv,
+):
+    me = lax.axis_index("sp")
+    rank = lax.axis_index("tp")
+    parity = lax.rem(rank, 2)
+    sibling = rank + 1 - 2 * parity
+    chips = tp_size // 2
+    chip = rank // 2
+    span = sp_size // groups
+    cap = outgoing.shape[1]
+    feats = outgoing.shape[2]
+    units = gate.shape[1]
+    columns = down.shape[1]
+
+    weights = [
+        pltpu.make_async_copy(src, dst, weight_sem.at[i])
+        for i, (src, dst) in enumerate(((gate_hbm, gate), (up_hbm, up), (down_hbm, down)))
+    ]
+    for copy in weights:
+        copy.start()
+
+    def peer_rank(step):
+        return lax.rem(chip + step, chips) * 2 + parity
+
+    barrier = pltpu.get_barrier_semaphore()
+    for step in range(1, sp_size):
+        pl.semaphore_signal(
+            barrier,
+            inc=1,
+            device_id={"sp": lax.rem(me + step, sp_size), "tp": rank},
+            device_id_type=pl.DeviceIdType.MESH,
+        )
+    for step in range(1, chips):
+        pl.semaphore_signal(
+            barrier,
+            inc=1,
+            device_id={"sp": me, "tp": peer_rank(step)},
+            device_id_type=pl.DeviceIdType.MESH,
+        )
+    pl.semaphore_signal(
+        barrier,
+        inc=1,
+        device_id={"sp": me, "tp": sibling},
+        device_id_type=pl.DeviceIdType.MESH,
+    )
+    pl.semaphore_wait(barrier, sp_size - 1 + chips)
+
+    def slot(step):
+        return rows_in.at[step // span, rank, pl.ds((step % span) * cap, cap)]
+
+    def dispatch(step):
+        expert = lax.rem(me + sp_size - step, sp_size)
+        return pltpu.make_async_remote_copy(
+            src_ref=outgoing.at[expert],
+            dst_ref=slot(step),
+            send_sem=disp_send.at[step],
+            recv_sem=disp_recv.at[step],
+            device_id={"sp": expert, "tp": rank},
+            device_id_type=pl.DeviceIdType.MESH,
+        )
+
+    own_in = pltpu.make_async_copy(outgoing.at[me], slot(0), local_sem.at[0])
+    own_in.start()
+    for step in range(1, sp_size):
+        dispatch(step).start()
+
+    def piece(buffer, send, recv, group, owner, target, send_slot):
+        return pltpu.make_async_remote_copy(
+            src_ref=buffer.at[group, owner],
+            dst_ref=buffer.at[group, owner],
+            send_sem=send.at[group, send_slot],
+            recv_sem=recv.at[group, owner],
+            device_id={"sp": me, "tp": target},
+            device_id_type=pl.DeviceIdType.MESH,
+        )
+
+    def spread(buffer, send, recv, group):
+        for step in range(1, chips):
+            target = peer_rank(step)
+            piece(buffer, send, recv, group, rank, target, target).start()
+        piece(buffer, send, recv, group, rank, sibling, sibling).start()
+
+    def collect(buffer, send, recv, group):
+        for step in range(1, chips):
+            owner = peer_rank(step)
+            forward = piece(buffer, send, recv, group, owner, sibling, owner + 1 - 2 * parity)
+            forward.wait_recv()
+            forward.start()
+        for step in range(chips):
+            owner = peer_rank(step) + 1 - 2 * parity
+            piece(buffer, send, recv, group, owner, sibling, sibling).wait_recv()
+
+    unit_tile = math.gcd(units, 256)
+    column_tile = math.gcd(columns, 256)
+
+    def spread_rows(group):
+        for place in range(span):
+            def arrived(place=place):
+                step = group * span + place
+                pltpu.make_async_remote_copy(
+                    src_ref=outgoing.at[0],
+                    dst_ref=rows_in.at[group, rank, pl.ds(place * cap, cap)],
+                    send_sem=disp_send.at[step],
+                    recv_sem=disp_recv.at[step],
+                    device_id={"sp": me, "tp": sibling},
+                    device_id_type=pl.DeviceIdType.MESH,
+                ).wait_recv()
+
+            if place == 0:
+                @pl.when(group == 0)
+                def _():
+                    own_in.wait()
+
+                pl.when(group > 0)(arrived)
+            else:
+                arrived()
+        spread(rows_in, row_send, row_recv, group)
+
+    def run_up(group):
+        collect(rows_in, row_send, row_recv, group)
+
+        @pl.when(group == 0)
+        def _():
+            weights[0].wait()
+            weights[1].wait()
+
+        @pl.loop(0, units // unit_tile)
+        def _(tile):
+            cols = pl.ds(pl.multiple_of(tile * unit_tile, unit_tile), unit_tile)
+            pre_gate = 0.0
+            pre_up = 0.0
+            for part in range(tp_size):
+                block = rows_in[group, part]
+                depth = pl.ds(part * feats, feats)
+                pre_gate += jnp.dot(block, gate[depth, cols], preferred_element_type=jnp.float32)
+                pre_up += jnp.dot(block, up[depth, cols], preferred_element_type=jnp.float32)
+            capped = jnp.minimum(pre_gate, CLAMP_LIMIT)
+            linear = jnp.clip(pre_up, -CLAMP_LIMIT, CLAMP_LIMIT)
+            value = capped * jax.nn.sigmoid(SWISH_ALPHA * capped) * (linear + 1.0)
+            hidden[group, rank, :, cols] = value.astype(jnp.bfloat16)
+
+        spread(hidden, hid_send, hid_recv, group)
+
+    def give_back(step):
+        source = lax.rem(me + step, sp_size)
+        return pltpu.make_async_remote_copy(
+            src_ref=result.at[step // span, pl.ds((step % span) * cap, cap)],
+            dst_ref=returned.at[me],
+            send_sem=ret_send.at[step],
+            recv_sem=ret_recv.at[step],
+            device_id={"sp": source, "tp": rank},
+            device_id_type=pl.DeviceIdType.MESH,
+        )
+
+    own_out = pltpu.make_async_copy(result.at[0, pl.ds(0, cap)], returned.at[me], local_sem.at[1])
+
+    def run_down(group):
+        collect(hidden, hid_send, hid_recv, group)
+
+        @pl.when(group == 0)
+        def _():
+            weights[2].wait()
+
+        @pl.loop(0, columns // column_tile)
+        def _(tile):
+            cols = pl.ds(pl.multiple_of(tile * column_tile, column_tile), column_tile)
+            total = 0.0
+            for part in range(tp_size):
+                total += jnp.dot(
+                    hidden[group, part],
+                    down[pl.ds(part * units, units), cols],
+                    preferred_element_type=jnp.float32,
+                )
+            result[group, :, cols] = total.astype(jnp.bfloat16)
+
+        for place in range(span):
+            if place == 0:
+                @pl.when(group == 0)
+                def _():
+                    own_out.start()
+
+                @pl.when(group > 0)
+                def _():
+                    give_back(group * span).start()
+            else:
+                give_back(group * span + place).start()
+
+    @pl.loop(0, groups + 2)
+    def _(turn):
+        @pl.when(turn < groups)
+        def _():
+            spread_rows(turn)
+
+        @pl.when((turn >= 1) & (turn < groups + 1))
+        def _():
+            run_up(turn - 1)
+
+        @pl.when(turn >= 2)
+        def _():
+            run_down(turn - 2)
+
+    own_out.wait()
+    for step in range(1, sp_size):
+        dispatch(step).wait_send()
+    for step in range(1, sp_size):
+        back = give_back(step)
+        back.wait_send()
+        pltpu.make_async_remote_copy(
+            src_ref=result.at[0, pl.ds(0, cap)],
+            dst_ref=returned.at[lax.rem(me + sp_size - step, sp_size)],
+            send_sem=ret_send.at[step],
+            recv_sem=ret_recv.at[step],
+            device_id={"sp": lax.rem(me + step, sp_size), "tp": rank},
+            device_id_type=pl.DeviceIdType.MESH,
+        ).wait_recv()
+
+    @pl.loop(0, groups)
+    def _(group):
+        for buffer, send, recv in ((rows_in, row_send, row_recv), (hidden, hid_send, hid_recv)):
+            for step in range(1, chips):
+                target = peer_rank(step)
+                piece(buffer, send, recv, group, rank, target, target).wait_send()
+                other = target + 1 - 2 * parity
+                piece(buffer, send, recv, group, target, sibling, other).wait_send()
+            piece(buffer, send, recv, group, rank, sibling, sibling).wait_send()
+
+
+def run_experts(outgoing, gate_weight, up_weight, down_weight):
+    sp_size, cap, feats = outgoing.shape
+    tp_size = lax.axis_size("tp")
+    groups = math.gcd(sp_size, 4)
+    rows = sp_size // groups * cap
+    units = gate_weight.shape[1]
+    columns = down_weight.shape[1]
+    dma = pltpu.SemaphoreType.DMA
+    return pl.pallas_call(
+        functools.partial(expert_kernel, sp_size, tp_size, groups),
+        out_shape=jax.ShapeDtypeStruct((sp_size, cap, columns), jnp.bfloat16),
+        in_specs=[pl.BlockSpec(memory_space=pltpu.VMEM)]
+        + [pl.BlockSpec(memory_space=pl.ANY)] * 3,
+        out_specs=pl.BlockSpec(memory_space=pl.ANY),
+        scratch_shapes=[
+            pltpu.VMEM((groups, tp_size, rows, feats), jnp.bfloat16),
+            pltpu.VMEM((groups, tp_size, rows, units), jnp.bfloat16),
+            pltpu.VMEM((groups, rows, columns), jnp.bfloat16),
+            pltpu.VMEM(gate_weight.shape, jnp.bfloat16),
+            pltpu.VMEM(up_weight.shape, jnp.bfloat16),
+            pltpu.VMEM(down_weight.shape, jnp.bfloat16),
+            dma((3,)),
+            dma((2,)),
+            dma((sp_size,)),
+            dma((sp_size,)),
+            dma((sp_size,)),
+            dma((sp_size,)),
+            dma((groups, tp_size)),
+            dma((groups, tp_size)),
+            dma((groups, tp_size)),
+            dma((groups, tp_size)),
+        ],
+        compiler_params=pltpu.CompilerParams(
+            collective_id=0, has_side_effects=True, vmem_limit_bytes=48 * 1024 * 1024
+        ),
+    )(outgoing, gate_weight, up_weight, down_weight)
 
 
 def local(
@@ -119,7 +411,7 @@
     )
     experts = lax.axis_size("sp")
     top_count = expert_ids.shape[1]
-    capacity = 2 * tokens_here * top_count // experts
+    capacity = -(-(2 * tokens_here * top_count // experts) // 16) * 16
     chosen = expert_ids.reshape(-1)
     onehot = (chosen[:, None] == jnp.arange(experts, dtype=jnp.int32)[None, :]).astype(jnp.int32)
     rank_in = jnp.sum(jnp.cumsum(onehot, axis=0) * onehot, axis=1) - 1
@@ -131,28 +423,7 @@
     )
     padded = jnp.concatenate([normed, jnp.zeros((1, normed.shape[1]), jnp.bfloat16)], axis=0)
     outgoing = padded[owner_row].reshape(experts, capacity, normed.shape[1])
-    expert_input = lax.all_gather(
-        lax.all_to_all(outgoing, "sp", split_axis=0, concat_axis=0, tiled=True),
-        "tp",
-        axis=2,
-        tiled=True,
-    )
-    sources = expert_input.shape[0]
-    items = expert_input.shape[1]
-    flat_rows = expert_input.reshape(sources * items, -1)
-    pre_gate = jnp.dot(flat_rows, gate_weight[0], preferred_element_type=jnp.float32)
-    pre_up = jnp.dot(flat_rows, up_weight[0], preferred_element_type=jnp.float32)
-    capped = jnp.minimum(pre_gate, CLAMP_LIMIT)
-    linear = jnp.clip(pre_up, -CLAMP_LIMIT, CLAMP_LIMIT)
-    hidden = (capped * jax.nn.sigmoid(SWISH_ALPHA * capped) * (linear + 1.0)).astype(jnp.bfloat16)
-    weight_slice = down_weight[0]
-    expert_out = jnp.dot(
-        lax.all_gather(hidden, "tp", axis=1, tiled=True),
-        weight_slice,
-        preferred_element_type=jnp.float32,
-    )
-    expert_out = expert_out.astype(jnp.bfloat16).reshape(sources, items, -1)
-    returned_rows = lax.all_to_all(expert_out, "sp", split_axis=0, concat_axis=0, tiled=True)
+    returned_rows = run_experts(outgoing, gate_weight[0], up_weight[0], down_weight[0])
     picked = returned_rows.reshape(experts * capacity, -1)[slot_index].astype(jnp.float32)
     picked = picked.reshape(tokens_here, top_count, -1)
     weights = jax.nn.softmax(route_logit, axis=-1)

time: 297 us -> 232 us (0.78)
  waiting for transfers between devices: 175 us -> 81.4 us
  Pallas kernels: 0 us -> 82.8 us
  blocking collectives: 47.2 us -> 14.9 us
  matrix products: 22.8 us -> 2.93 us
  starting transfers between devices: 5.96 us -> 0.08 us
  local copies, waits for them, and re-layouts: 24.5 us -> 28.4 us
    pallas_call x0 -> x1, Pallas kernels: none -> 82.8 us  [run_experts(): pl.pallas_call(functools.partial(expert_kernel, sp_size, tp_size, groups)...]
    all_gather x2 -> x0, waiting for transfers between devices: 73 us -> none  [the longest x1 46.5 us: local(): lax.all_gather(hidden, 'tp', axis=1, tiled=True)]
    all_to_all x1 -> x0, blocking collectives: 32.5 us -> none  [local(): lax.all_to_all(outgoing, 'sp', split_axis=0, concat_axis=0, tiled=True)]
    all_to_all x1 -> x0, waiting for transfers between devices: 20.4 us -> none  [local(): lax.all_to_all(expert_out, 'sp', split_axis=0, concat_axis=0, tiled=True)]
    dot_general x3 -> x0, matrix products: 19.9 us -> none  [the longest x1 8.3 us: local(): jnp.dot(lax.all_gather(hidden, 'tp', axis=1, tiled=True), weight_slice, p...]
    all_to_all x1 -> x0, starting transfers between devices: 5.65 us -> none  [local(): lax.all_to_all(expert_out, 'sp', split_axis=0, concat_axis=0, tiled=True)]
    unnamed x25, local copies, waits for them, and re-layouts: 9.82 us -> 13.2 us
  transfers between devices with their start and end apart: 5 -> 2, of which waited for: 5 -> 2; matrix products, arithmetic and copies ran while one was open for 4% -> 5% of each run, Pallas kernels for 0% -> 0%
where the time goes in v1:
time: 232 us
  Pallas kernels  82.8 us (36%)
  waiting for transfers between devices  81.4 us (35%)
  local copies, waits for them, and re-layouts  28.4 us (12%)
  blocking collectives  14.9 us (6%)
  between operations  13.7 us (6%)
  other arithmetic  5.08 us (2%)
  matrix products  2.93 us (1%)
    pallas_call x1, Pallas kernels, run_experts(): pl.pallas_call(functools.partial(expert_kernel, sp_size, tp_size, groups)...  82.8 us
    all_gather x1, waiting for transfers between devices, local(): value_piece = lax.all_gather(value_rows, 'sp', axis=0, tiled=True)  42.2 us
    all_gather x1, waiting for transfers between devices, local(): key_piece = lax.all_gather(key_rows, 'sp', axis=0, tiled=True)  39.2 us
    unnamed x25, local copies, waits for them, and re-layouts  13.2 us
    all_gather x1, blocking collectives, local(): lax.all_gather(attended, 'tp', axis=0, tiled=True)  8.58 us
    psum x1, blocking collectives, local(): square_total = lax.psum(partial_value, 'tp')  6.34 us
  transfers between devices with their start and end apart: 2, of which 2 were waited for; matrix products, arithmetic and copies ran while one was open for 5% of the time, Pallas kernels for 0%

profile of v1, /device:TPU:0, one launch (start us, length us, event | category | flops | bytes accessed | tf_op | source)
XLA Modules:
  0.0 231.6 jit_solution(15255593520062161190)
XLA Ops:
  6.5 0.0 copy-start
  6.5 0.0 copy-start.7
  6.5 0.0 all-gather.3.cloned.1.call-start
  6.6 1.8 copy.27
  8.4 0.0 all-gather.3.cloned.1.call-update
  8.4 0.0 all-gather.5.cloned.1.call-start
  8.5 1.6 copy.29
  10.1 0.0 all-gather.5.cloned.1.call-update
  10.2 0.8 copy.34
  11.0 0.1 eq.29
  11.1 0.1 eq.25
  11.2 0.0 copy-done.4
  11.3 0.2 fusion.45
  11.5 0.1 copy.37
  11.6 0.1 copy.38
  11.8 0.9 reduce-window.6
  12.7 0.2 slice_reduce_fusion
  12.9 0.0 copy-done.7
  12.9 0.1 copy.33
  13.0 0.1 mul.161
  13.2 0.0 copy-done.6
  13.3 0.1 copy.36
  13.4 0.8 dynamic_slice.28
  14.2 0.1 fusion.33
  14.3 2.9 %scatter_custom_fusion = s32[768]{0:T(1024)S(1)} fusion(s32[384]{0:T(512)S(1)} %fusion.40, s32[384]{0:T(512)S(1)} %add_select_fusion.1, s32[]{:T(128)} %constant.135.clone.1), kind=kCustom, calls=%fused_computation.82 | custom fusion | bytes 3076 | tf_op jit(solution)/shard_map/scatter | solution.py:422
  17.3 39.2 %all-gather.3.cloned.1.call-done = bf16[1536,4,128]{2,0,1:T(8,128)(2,1)} async-done(((bf16[192,4,128]{2,0,1:T(8,128)(2,1)}), bf16[1536,4,128]{2,0,1:T(8,128)(2,1)}) %all-gather.3.cloned.1.call-update) | async-done | bytes 1572880 | tf_op jit(solution)/shard_map/all_gather | solution.py:359
  56.5 2.6 %copy.31 = bf16[3,512,4,128]{1,3,2,0:T(8,128)(2,1)} copy(bf16[3,512,4,128]{3,1,0,2:T(8,128)(2,1)} %bitcast.51) | data formatting | bytes 3145728
  59.1 42.2 %all-gather.5.cloned.1.call-done = bf16[1536,4,128]{2,0,1:T(8,128)(2,1)} async-done(((bf16[192,4,128]{2,0,1:T(8,128)(2,1)}), bf16[1536,4,128]{2,0,1:T(8,128)(2,1)}) %all-gather.5.cloned.1.call-update) | async-done | bytes 1572880 | tf_op jit(solution)/shard_map/all_gather | solution.py:360
  101.3 2.7 %copy.32 = bf16[3,512,4,128]{3,1,2,0:T(8,128)(2,1)} copy(bf16[3,512,4,128]{3,1,0,2:T(8,128)(2,1)} %bitcast.52) | data formatting | bytes 3145728
  104.0 0.0 copy-start.8
  104.0 0.0 copy-start.9
  104.0 9.0 %while.23 = (s32[]{:T(128)}, f32[4,192]{1,0:T(4,128)S(1)}, f32[4,192]{1,0:T(4,128)S(1)}, f32[4,192,128]{2,1,0:T(8,128)S(1)}, f32[4,192]{1,0:T(4,128)S(1)}, /*ind...) while((s32[]{:T(128)}, f32[4,192]{1,0:T(4,128)S(1)}, ...), condition=%wide.region_7.8_spmd.clone, body=%wide.region_0.7_spmd.clone.sunk | while | flops 309574784 | bytes 20891532 | solution.py:383
  104.1 0.6 dynamic_slice.42
  105.4 5.0 %conditional.3 = ((f32[4,192]{1,0:T(4,128)S(1)}, f32[4,192]{1,0:T(4,128)S(1)}, f32[4,192,128]{2,1,0:T(8,128)S(1)}, f32[4,192]{1,0:T(4,128)S(1)}, f32[4,192]{1,0:T(4,128)S(1)}, /*index=5*/f32[4,192,128]{2,1,0:T(8,128)S(1)})) conditional(s32[]{:T(128)} %convert_element_type.72, (f32[4,192]{1,0:T(4,128)S(1)}, f32[4,192]{1,0:T(4,128)S(1)}, ...), branch_computations={%region_1.1_spmd, %region_2.6_spmd.clone} | conditional | flops 309572096 | bytes 20887848 | solution.py:378
  105.4 0.1 broadcast_compare_fusion
  105.5 1.1 dynamic-slice_bitcast_fusion
  106.6 0.6 fusion.43
  107.2 0.6 fusion.44
  107.8 0.0 copy-start.3
  107.8 1.2 fusion.5
  109.0 0.2 copy-done.3
  109.2 0.6 convolution_add_fusion
  109.7 0.6 convolution_add_fusion.1
  110.4 0.6 dynamic_slice.42
  111.7 0.6 dynamic_slice.42
  113.0 0.0 copy-start.5
  113.0 0.0 copy-done.8
  113.0 0.5 multiply_reduce_fusion.2
  113.5 0.0 copy-done.9
  113.6 0.2 multiply_convert_fusion.1
  113.7 8.6 %all_gather.11 = bf16[16,192,128]{2,1,0:T(8,128)(2,1)S(1)} all-gather(bf16[4,192,128]{2,1,0:T(8,128)(2,1)S(1)} %multiply_convert_fusion.1), channel_id=1, replica_groups=mesh['sp'=8,'tp'=4] {'tp'}, dimensions={0}, use_global_device_ids=true | all-gather | bytes 983040 | tf_op jit(solution)/shard_map/all_gather | solution.py:398
  122.3 0.0 copy-done
  122.3 0.0 copy-done.5
  122.3 0.7 multiply_reduce_fusion.1
  123.0 6.3 %psum.7 = f32[192]{0:T(256)S(1)} all-reduce(f32[192]{0:T(256)S(1)} %get-tuple-element.467), channel_id=1, replica_groups=mesh['sp'=8,'tp'=4] {'tp'}, use_global_device_ids=true, to_apply=%region_10.11 | all-reduce | flops 192 | bytes 1536 | tf_op jit(solution)/shard_map/psum | solution.py:405
  129.3 0.1 multiply_convert_fusion
  129.5 3.3 %gather_fusion = bf16[768,512]{1,0:T(8,128)(2,1)} fusion(bf16[193,512]{1,0:T(8,128)(2,1)S(1)} %concatenate.3, s32[1024]{0:T(1024)S(1)} %pad_clamp_fusion.1), kind=kCustom, calls=%fused_computation | custom fusion | bytes 1575936 | tf_op jit(solution)/shard_map/gather | solution.py:425
  132.8 2.2 copy-done.1
  135.0 1.1 copy-done.2
  136.1 82.8 %shard_map.127 = bf16[8,96,512]{2,1,0:T(8,128)(2,1)S(1)} custom-call(bf16[8,96,512]{2,1,0:T(8,128)(2,1)S(1)} %bitcast.48, bf16[2048,1024]{1,0:T(8,128)(2,1)S(1)} %bitcast.47, bf16[2048,1024]{1,0:T(8,128)(2,1)} %bitcast.49, bf16[4096,512]{1,0:T(8,128)(2,1)} %bitcast.50), custom_call_target="tpu_custom_call" | custom-call | tf_op jit(solution)/shard_map/pallas_call | solution.py:301
  218.9 2.6 %gather_fusion.1 = bf16[384,512]{1,0:T(8,128)(2,1)} fusion(bf16[768,512]{1,0:T(8,128)(2,1)S(1)} %bitcast.46, s32[1024]{0:T(1024)S(1)} %pad_clamp_fusion), kind=kCustom, calls=%fused_computation.1 | custom fusion | bytes 787968 | tf_op jit(solution)/shard_map/gather | solution.py:427
  221.5 1.5 reshape.145
  223.0 1.0 multiply_reduce_fusion
  224.0 0.7 add_convert_fusion
  (47 shorter events, 0.4 us)
Async XLA Ops:
  6.5 115.8 %copy-start = (bf16[2048,512]{1,0:T(8,128)(2,1)S(1)}, bf16[2048,512]{1,0:T(8,128)(2,1)}, u32[]{:S(2)}) copy-start(bf16[2048,512]{1,0:T(8,128)(2,1)} %param.23) | copy-start | bytes 6291460
  6.5 6.4 %copy-start.7 = (s32[192,2]{0,1:T(2,128)S(1)}, s32[192,2]{0,1:T(2,128)}, u32[]{:S(2)}) copy-start(s32[192,2]{0,1:T(2,128)} %param.28) | copy-start | bytes 4612
  6.5 4.7 %copy-start.4 = (bf16[192,4,128]{2,1,0:T(4,128)(2,1)S(1)}, bf16[192,4,128]{2,1,0:T(4,128)(2,1)}, u32[]{:S(2)}) copy-start(bf16[192,4,128]{2,1,0:T(4,128)(2,1)} %param.18) | copy-start | bytes 589828
  6.5 6.7 %copy-start.6 = (f32[192,2]{0,1:T(2,128)S(1)}, f32[192,2]{0,1:T(2,128)}, u32[]{:S(2)}) copy-start(f32[192,2]{0,1:T(2,128)} %param.29) | copy-start | bytes 4612
  6.5 49.9 %all-gather.3.cloned.1.call-start = ((), (), s32[]{:S(2)}) async-start(), calls=%async_computation | async-start | bytes 1769472 | tf_op jit(solution)/shard_map/all_gather | solution.py:359
  8.4 92.8 %all-gather.5.cloned.1.call-start = ((), (), s32[]{:S(2)}) async-start(), calls=%async_computation.1 | async-start | bytes 1769472 | tf_op jit(solution)/shard_map/all_gather | solution.py:360
  104.0 9.0 %copy-start.8 = (f32[4]{0:T(128)S(1)}, f32[4]{0:T(128)}, u32[]{:S(2)}) copy-start(f32[4]{0:T(128)} %param.21) | copy-start | bytes 52
  104.0 9.5 %copy-start.9 = (f32[128]{0:T(128)S(1)}, f32[128]{0:T(128)}, u32[]{:S(2)}) copy-start(f32[128]{0:T(128)} %param.22) | copy-start | bytes 1540
  107.8 1.4 copy-start.3
  113.0 9.3 %copy-start.5 = (bf16[192,512]{1,0:T(8,128)(2,1)S(1)}, bf16[192,512]{1,0:T(8,128)(2,1)}, u32[]{:S(2)}) copy-start(bf16[192,512]{1,0:T(8,128)(2,1)} %param.17) | copy-start | bytes 589828
  132.8 2.2 copy-start.1
  135.0 1.1 copy-start.2
Sparse Core Ops, SparseCore 0:
  9.5 46.9 all-gather.2
  58.7 42.5 all-gather.4

commit v2 on v1

--- a/solution.py
+++ b/solution.py
@@ -20,23 +20,181 @@
 NEG_FILL = -1e30
 
 
-def update_map(running, query_half, key_half, value_block, visible):
-    row_peak, row_total, accum = running
-    scores = jnp.einsum(
-        "qhd,khd->hqk", query_half, key_half, preferred_element_type=jnp.float32
-    ) * QK ** (-0.5)
-    scores = jnp.where(visible[None], scores, NEG_FILL)
-    new_peak = jnp.maximum(row_peak, jnp.max(scores, axis=-1))
-    exp_weights = jnp.where(visible[None], jnp.exp(scores - new_peak[..., None]), 0.0)
-    rescale = jnp.exp(row_peak - new_peak)
-    row_total = row_total * rescale + jnp.sum(exp_weights, axis=-1)
-    accum = accum * rescale[..., None] + jnp.einsum(
-        "hqk,khv->hqv",
-        exp_weights.astype(jnp.bfloat16),
-        value_block,
-        preferred_element_type=jnp.float32,
-    )
-    return (new_peak, row_total, accum)
+def attend_kernel(
+    sp_size,
+    queries,
+    own_block,
+    diff_scale,
+    head_gain,
+    attended,
+    blocks,
+    peak,
+    total,
+    accum,
+    local_sem,
+    along_send,
+    across_send,
+    recv,
+):
+    me = lax.axis_index("sp")
+    rank = lax.axis_index("tp")
+    pairs = sp_size // 2
+    pair = me // 2
+    side = lax.rem(me, 2)
+    other = me + 1 - 2 * side
+    tokens = queries.shape[0]
+    width = head_gain.shape[1]
+    heads = queries.shape[1] // width
+
+    def place(index):
+        return {"sp": index, "tp": rank}
+
+    load = pltpu.make_async_copy(own_block, blocks.at[me], local_sem)
+    load.start()
+    barrier = pltpu.get_barrier_semaphore()
+
+    def greet(index):
+        pl.semaphore_signal(
+            barrier, inc=1, device_id=place(index), device_id_type=pl.DeviceIdType.MESH
+        )
+
+    greet(other)
+
+    @pl.when(pair > 0)
+    def _():
+        greet(me - 2)
+
+    @pl.when(pair < pairs - 1)
+    def _():
+        greet(me + 2)
+
+    pl.semaphore_wait(barrier, 1 + jnp.minimum(pair, 1) + jnp.minimum(pairs - 1 - pair, 1))
+    peak[...] = jnp.full(peak.shape, NEG_FILL, jnp.float32)
+    total[...] = jnp.zeros(total.shape, jnp.float32)
+    accum[...] = jnp.zeros(accum.shape, jnp.float32)
+    load.wait()
+
+    def hand_on(block, send, back, target):
+        return pltpu.make_async_remote_copy(
+            src_ref=blocks.at[block],
+            dst_ref=blocks.at[block],
+            send_sem=send.at[back],
+            recv_sem=recv.at[block],
+            device_id=place(target),
+            device_id_type=pl.DeviceIdType.MESH,
+        )
+
+    def compute(block):
+        row = me * tokens + lax.broadcasted_iota(jnp.int32, (tokens, tokens), 0)
+        col = block * tokens + lax.broadcasted_iota(jnp.int32, (tokens, tokens), 1)
+        visible = col // SPAN <= row // SPAN
+        for head in range(heads):
+            value = blocks[block, 1, :, head * width : (head + 1) * width]
+            for half in range(2):
+                start = head * width + half * QK
+                scores = lax.dot_general(
+                    queries[:, start : start + QK],
+                    blocks[block, 0, :, start : start + QK],
+                    (((1,), (1,)), ((), ())),
+                    preferred_element_type=jnp.float32,
+                ) * QK ** (-0.5)
+                scores = jnp.where(visible, scores, NEG_FILL)
+                index = head * 2 + half
+                old = peak[index]
+                new = jnp.maximum(old, jnp.max(scores, axis=-1, keepdims=True))
+                weights = jnp.where(visible, jnp.exp(scores - new), 0.0)
+                rescale = jnp.exp(old - new)
+                peak[index] = new
+                total[index] = total[index] * rescale + jnp.sum(weights, axis=-1, keepdims=True)
+                accum[index] = accum[index] * rescale + jnp.dot(
+                    weights.astype(jnp.bfloat16), value, preferred_element_type=jnp.float32
+                )
+
+    @pl.loop(0, pair + 2)
+    def _(back):
+        @pl.when(back <= pair)
+        def _():
+            block = me - 2 * back
+
+            @pl.when(back > 0)
+            def _():
+                hand_on(block, across_send, back, other).wait_recv()
+
+            @pl.when(pair < pairs - 1)
+            def _():
+                hand_on(block, along_send, back, me + 2).start()
+
+            @pl.when((back > 0) | (side == 0))
+            def _():
+                hand_on(block, across_send, back, other).start()
+
+        second = other - 2 * (back - 1)
+        use_second = (back >= 2) | ((back == 1) & (side == 1))
+
+        @pl.loop(0, 2)
+        def _(which):
+            @pl.when((which == 1) & use_second)
+            def _():
+                hand_on(second, across_send, 0, other).wait_recv()
+
+            @pl.when(((which == 0) & (back <= pair)) | ((which == 1) & use_second))
+            def _():
+                compute(jnp.where(which == 0, me - 2 * back, second))
+
+    for head in range(heads):
+        first = accum[head * 2] / total[head * 2]
+        later = accum[head * 2 + 1] / total[head * 2 + 1]
+        mixture = first - diff_scale[head] * later
+        scale_back = lax.rsqrt(jnp.mean(mixture * mixture, axis=-1, keepdims=True) + NORM_EPS)
+        attended[:, head * width : (head + 1) * width] = (
+            mixture * scale_back * head_gain[...] * HEAD_KEEP
+        ).astype(jnp.bfloat16)
+
+    @pl.loop(0, pair + 1)
+    def _(back):
+        block = me - 2 * back
+
+        @pl.when(pair < pairs - 1)
+        def _():
+            hand_on(block, along_send, back, me + 2).wait_send()
+
+        @pl.when((back > 0) | (side == 0))
+        def _():
+            hand_on(block, across_send, back, other).wait_send()
+
+
+def run_attention(queries, key_rows, value_rows, diff_scale, head_gain):
+    sp_size = lax.axis_size("sp")
+    tokens, heads, width = value_rows.shape
+    own_block = jnp.stack(
+        [key_rows.reshape(tokens, heads * width), value_rows.reshape(tokens, heads * width)]
+    )
+    dma = pltpu.SemaphoreType.DMA
+    vmem = pl.BlockSpec(memory_space=pltpu.VMEM)
+    return pl.pallas_call(
+        functools.partial(attend_kernel, sp_size),
+        out_shape=jax.ShapeDtypeStruct((tokens, heads * width), jnp.bfloat16),
+        in_specs=[
+            vmem,
+            pl.BlockSpec(memory_space=pl.ANY),
+            pl.BlockSpec(memory_space=pltpu.SMEM),
+            vmem,
+        ],
+        out_specs=vmem,
+        scratch_shapes=[
+            pltpu.VMEM((sp_size,) + own_block.shape, jnp.bfloat16),
+            pltpu.VMEM((heads * 2, tokens, 1), jnp.float32),
+            pltpu.VMEM((heads * 2, tokens, 1), jnp.float32),
+            pltpu.VMEM((heads * 2, tokens, width), jnp.float32),
+            dma(()),
+            dma((sp_size,)),
+            dma((sp_size,)),
+            dma((sp_size,)),
+        ],
+        compiler_params=pltpu.CompilerParams(
+            collective_id=1, has_side_effects=True, vmem_limit_bytes=32 * 1024 * 1024
+        ),
+    )(queries.reshape(tokens, heads * width), own_block, diff_scale, head_gain[None])
 
 
 def expert_kernel(
@@ -344,59 +502,13 @@
     route_logit,
 ):
     tokens_here = queries.shape[0]
-    heads_here = queries.shape[1]
-    value_width = value_rows.shape[2]
-    query_start = lax.axis_index("sp") * tokens_here
-    query_span = (query_start + jnp.arange(tokens_here, dtype=jnp.int32)) // SPAN
-    first_query = queries[..., :QK]
-    second_query = queries[..., QK:]
-    empty_map = (
-        jnp.full((heads_here, tokens_here), NEG_FILL, jnp.float32),
-        jnp.zeros((heads_here, tokens_here), jnp.float32),
-        jnp.zeros((heads_here, tokens_here, value_width), jnp.float32),
-    )
-    folded = (empty_map, empty_map)
-    key_piece = lax.all_gather(key_rows, "sp", axis=0, tiled=True)
-    value_piece = lax.all_gather(value_rows, "sp", axis=0, tiled=True)
-    key_count = key_piece.shape[0]
-    key_width = math.gcd(key_count, 1024)
-    blocks = key_count // key_width
-    key_blocks = key_piece.reshape(blocks, key_width, heads_here, 2 * QK)
-    value_blocks = value_piece.reshape(blocks, key_width, heads_here, value_width)
-
-    def advance(running, inputs):
-        block_index, key_block, value_block = inputs
-        key_start = block_index * key_width
-
-        def compute(current):
-            key_span = (key_start + jnp.arange(key_width, dtype=jnp.int32)) // SPAN
-            visible = key_span[None, :] <= query_span[:, None]
-            first = update_map(current[0], first_query, key_block[..., :QK], value_block, visible)
-            second = update_map(current[1], second_query, key_block[..., QK:], value_block, visible)
-            return (first, second)
-
-        running = lax.cond(
-            key_start < query_start + tokens_here, compute, lambda current: current, running
-        )
-        return (running, None)
-
-    folded, _ = lax.scan(
-        advance, folded, (jnp.arange(blocks, dtype=jnp.int32), key_blocks, value_blocks)
-    )
-    first_map, second_map = folded
-    mixture = (
-        first_map[2] / first_map[1][..., None]
-        - diff_scale[:, None, None] * second_map[2] / second_map[1][..., None]
-    )
-    scale_back = lax.rsqrt(jnp.mean(mixture * mixture, axis=-1, keepdims=True) + NORM_EPS)
-    attended = (mixture * scale_back * head_gain * HEAD_KEEP).astype(jnp.bfloat16)
+    attended = run_attention(queries, key_rows, value_rows, diff_scale, head_gain)
     column_width = out_weight.shape[1]
-    head_weight = out_weight.reshape(-1, value_width, column_width)
-    weight_slice = head_weight
+    gathered = lax.all_gather(attended, "tp", axis=0)
     projected = jnp.einsum(
-        "htv,hvd->td",
-        lax.all_gather(attended, "tp", axis=0, tiled=True),
-        weight_slice,
+        "rtv,rvd->td",
+        gathered,
+        out_weight.reshape(gathered.shape[0], -1, column_width),
         preferred_element_type=jnp.float32,
     )
     after_mixer = (residual.astype(jnp.float32) + projected).astype(jnp.bfloat16)
@@ -413,21 +525,32 @@
     top_count = expert_ids.shape[1]
     capacity = -(-(2 * tokens_here * top_count // experts) // 16) * 16
     chosen = expert_ids.reshape(-1)
-    onehot = (chosen[:, None] == jnp.arange(experts, dtype=jnp.int32)[None, :]).astype(jnp.int32)
-    rank_in = jnp.sum(jnp.cumsum(onehot, axis=0) * onehot, axis=1) - 1
-    slot_index = chosen * capacity + rank_in
-    owner_row = (
-        jnp.full((experts * capacity,), tokens_here, jnp.int32)
-        .at[slot_index]
-        .set(jnp.arange(tokens_here * top_count, dtype=jnp.int32) // top_count)
-    )
-    padded = jnp.concatenate([normed, jnp.zeros((1, normed.shape[1]), jnp.bfloat16)], axis=0)
-    outgoing = padded[owner_row].reshape(experts, capacity, normed.shape[1])
+    order = jnp.arange(chosen.shape[0], dtype=jnp.int32)
+    earlier = (chosen[:, None] == chosen[None, :]) & (order[None, :] < order[:, None])
+    rank_in = jnp.sum(earlier.astype(jnp.int32), axis=1)
+    slot_index = (chosen * capacity + rank_in).reshape(tokens_here, top_count)
+    slots = jnp.arange(experts * capacity, dtype=jnp.int32)
+    holds = [slot_index[:, k][:, None] == slots[None, :] for k in range(top_count)]
+    holds_any = functools.reduce(jnp.logical_or, holds)
+    outgoing = (
+        jnp.einsum(
+            "ts,td->sd",
+            holds_any.astype(jnp.bfloat16),
+            normed,
+            preferred_element_type=jnp.float32,
+        )
+        .astype(jnp.bfloat16)
+        .reshape(experts, capacity, normed.shape[1])
+    )
     returned_rows = run_experts(outgoing, gate_weight[0], up_weight[0], down_weight[0])
-    picked = returned_rows.reshape(experts * capacity, -1)[slot_index].astype(jnp.float32)
-    picked = picked.reshape(tokens_here, top_count, -1)
+    flat_rows = returned_rows.reshape(experts * capacity, -1)
     weights = jax.nn.softmax(route_logit, axis=-1)
-    routed = jnp.sum(picked * weights[..., None], axis=1)
+    routed = 0.0
+    for k in range(top_count):
+        picked = jnp.dot(
+            holds[k].astype(jnp.bfloat16), flat_rows, preferred_element_type=jnp.float32
+        )
+        routed = routed + picked * weights[:, k : k + 1]
     return (mixer_float + routed).astype(jnp.bfloat16)
 
 

time: 232 us -> 145 us (0.62)
  waiting for transfers between devices: 81.4 us -> 0 us
  Pallas kernels: 82.8 us -> 119 us
  local copies, waits for them, and re-layouts: 28.4 us -> 7.88 us
  between operations: 13.7 us -> 0.12 us
  other arithmetic: 5.08 us -> 0.35 us
    all_gather x2 -> x0, waiting for transfers between devices: 81.4 us -> none  [the longest x1 42.2 us: local(): value_piece = lax.all_gather(value_rows, 'sp', axis=0, tiled=True)]
    pallas_call x1, Pallas kernels: 82.8 us -> 106 us  [run_experts(): pl.pallas_call(functools.partial(expert_kernel, sp_size, tp_size, groups)...]
    pallas_call x0 -> x1, Pallas kernels: none -> 12.6 us  [run_attention(): pl.pallas_call(functools.partial(attend_kernel, sp_size), out_shape=jax.S...]
    unnamed x25 -> x16, local copies, waits for them, and re-layouts: 13.2 us -> 4.58 us
    gather x2 -> x0, local copies, waits for them, and re-layouts: 5.91 us -> none  [the longest x1 3.32 us: local(): outgoing = padded[owner_row].reshape(experts, capacity, normed.shape[1])]
    scatter x1 -> x0, local copies, waits for them, and re-layouts: 2.92 us -> none  [local(): owner_row = jnp.full((experts * capacity,), tokens_here, jnp.int32).at[sl...]
    reduce_sum x4 -> x1, other arithmetic: 2.78 us -> 0.24 us  [local(): rank_in = jnp.sum(earlier.astype(jnp.int32), axis=1)]
  transfers between devices with their start and end apart: 2 -> 0, of which waited for: 2 -> 0; matrix products, arithmetic and copies ran while one was open for 5% -> 0% of each run, Pallas kernels for 0% -> 0%
where the time goes in v2:
time: 145 us; the launch traced here: 144 us
  Pallas kernels  119 us (82%)
  blocking collectives  14.7 us (10%)
  local copies, waits for them, and re-layouts  7.88 us (5%)
  matrix products  2.65 us (2%)
    pallas_call x1, Pallas kernels, run_experts(): pl.pallas_call(functools.partial(expert_kernel, sp_size, tp_size, groups)...  106 us
    pallas_call x1, Pallas kernels, run_attention(): pl.pallas_call(functools.partial(attend_kernel, sp_size), out_shape=jax.S...  12.6 us
    all_gather x1, blocking collectives, local(): gathered = lax.all_gather(attended, 'tp', axis=0)  8.63 us
    psum x1, blocking collectives, local(): square_total = lax.psum(partial_value, 'tp')  6.12 us
    unnamed x16, local copies, waits for them, and re-layouts  4.58 us

profile of v2, /device:TPU:0, one launch (start us, length us, event | category | flops | bytes accessed | tf_op | source)
XLA Modules:
  0.0 144.3 jit_solution(14924185588422604546)
XLA Ops:
  0.0 0.0 copy-start
  0.0 0.0 copy-start.4
  0.0 0.9 dynamic_slice.3
  0.9 1.0 stack_reshape.6
  1.9 1.0 stack_reshape.7
  3.0 1.0 copy.27
  3.9 0.0 copy-start.2
  4.0 0.6 copy-done.2
  4.6 0.0 copy-start.3
  4.6 0.7 copy-done.3
  5.3 12.6 %shard_map.127 = bf16[192,512]{1,0:T(8,128)(2,1)S(1)} custom-call(bf16[192,512]{1,0:T(8,128)(2,1)S(1)} %bitcast.33, bf16[2,192,512]{2,1,0:T(8,128)(2,1)S(1)} %pad_maximum_fusion.own_block, f32[4]{0:T(128)S(1)} %copy-done.2, f32[1,128]{1,0:T(1,128)S(1)} %bitcast.34), custom_call_target="tpu_custom_call" | custom-call | tf_op jit(solution)/shard_map/pallas_call | solution.py:174
  17.8 0.0 copy-start.6
  17.9 8.6 %all-gather = bf16[768,512]{1,0:T(8,128)(2,1)S(1)} all-gather(bf16[192,512]{1,0:T(8,128)(2,1)S(1)} %shard_map.127), channel_id=2, replica_groups=mesh['sp'=8,'tp'=4] {'tp'}, dimensions={0}, use_global_device_ids=true | all-gather | bytes 983040 | tf_op jit(solution)/shard_map/all_gather | solution.py:507
  26.5 0.0 copy-done
  26.5 0.0 copy-done.4
  26.5 0.7 multiply_reduce_fusion
  27.2 0.0 copy-done.6
  27.2 0.1 copy.23
  27.3 0.1 eq.45
  27.4 0.2 convert_reduce_fusion
  27.7 0.1 reduce_sum.30
  27.8 0.1 copy.24
  27.9 6.1 %psum.7 = f32[192]{0:T(256)S(1)} all-reduce(f32[192]{0:T(256)S(1)} %get-tuple-element.9), channel_id=1, replica_groups=mesh['sp'=8,'tp'=4] {'tp'}, use_global_device_ids=true, to_apply=%region_2.0 | all-reduce | flops 192 | bytes 1536 | tf_op jit(solution)/shard_map/psum | solution.py:517
  34.1 0.5 convolution_convert_fusion
  34.6 0.0 copy-start.1
  34.6 2.2 %copy-done.1 = bf16[1,2048,1024]{2,1,0:T(8,128)(2,1)S(1)} copy-done((bf16[1,2048,1024]{2,1,0:T(8,128)(2,1)S(1)}, bf16[1,2048,1024]{2,1,0:T(8,128)(2,1)}, u32[]{:S(2)}) %copy-start.1) | copy-done | bytes 4194328
  36.8 0.0 copy-start.5
  36.8 106.0 %shard_map.128 = bf16[8,96,512]{2,1,0:T(8,128)(2,1)S(1)} custom-call(bf16[8,96,512]{2,1,0:T(8,128)(2,1)S(1)} %bitcast.32, bf16[2048,1024]{1,0:T(8,128)(2,1)S(1)} %bitcast.31, bf16[2048,1024]{1,0:T(8,128)(2,1)} %bitcast.35, bf16[4096,512]{1,0:T(8,128)(2,1)} %bitcast.36), custom_call_target="tpu_custom_call" | custom-call | tf_op jit(solution)/shard_map/pallas_call | solution.py:459
  142.8 0.0 copy-done.5
  142.9 0.4 convolution_multiply_fusion.1
  143.3 1.1 fusion.3
  (8 shorter events, 0.1 us)
Async XLA Ops:
  0.0 26.5 %copy-start = (bf16[2048,512]{1,0:T(8,128)(2,1)S(1)}, bf16[2048,512]{1,0:T(8,128)(2,1)}, u32[]{:S(2)}) copy-start(bf16[2048,512]{1,0:T(8,128)(2,1)} %param.19) | copy-start | bytes 6291460
  0.0 26.5 %copy-start.4 = (bf16[192,512]{1,0:T(8,128)(2,1)S(1)}, bf16[192,512]{1,0:T(8,128)(2,1)}, u32[]{:S(2)}) copy-start(bf16[192,512]{1,0:T(8,128)(2,1)} %param.13) | copy-start | bytes 589828
  3.9 0.7 copy-start.2
  4.6 0.7 copy-start.3
  17.8 9.3 %copy-start.6 = (s32[192,2]{0,1:T(2,128)S(1)}, s32[192,2]{0,1:T(2,128)}, u32[]{:S(2)}) copy-start(s32[192,2]{0,1:T(2,128)} %param.24) | copy-start | bytes 4612
  34.6 2.2 %copy-start.1 = (bf16[1,2048,1024]{2,1,0:T(8,128)(2,1)S(1)}, bf16[1,2048,1024]{2,1,0:T(8,128)(2,1)}, u32[]{:S(2)}) copy-start(bf16[1,2048,1024]{2,1,0:T(8,128)(2,1)} %param.21) | copy-start | bytes 12582916
  36.8 106.0 %copy-start.5 = (f32[192,2]{0,1:T(2,128)S(1)}, f32[192,2]{0,1:T(2,128)}, u32[]{:S(2)}) copy-start(f32[192,2]{0,1:T(2,128)} %param.25) | copy-start | bytes 4612
